TPU v7x, 512 devices: a whole 4x4x16 slice. The times are simulated.
512 devices in a mesh: fs: 16 (over y, x), tp: 32 (over z, core).
Axes of the slice: x: 4, y: 4, z: 16, core: 2. Of those that a mesh axis runs over, the one named last changes fastest.
Arguments:
- tokens: bfloat16 [16384, 2048], P(('fs', 'tp')), may hold values from -6 to 6
- norm_gain: float32 [2048], P('fs'), may hold values from 0.1 to 1.9
- gate_master: float32 [2048, 8192], P('fs', 'tp'), may hold values from -0.125 to 0.125
- up_master: float32 [2048, 8192], P('fs', 'tp'), may hold values from -0.125 to 0.125
- down_master: float32 [2048, 8192], P('fs', 'tp'), may hold values from -0.125 to 0.125
Outputs:
- mixed: bfloat16 [16384, 2048], P(('fs', 'tp'))
- gate_ready: bfloat16 [2048, 8192], P(None, 'tp')
- up_ready: bfloat16 [2048, 8192], P(None, 'tp')
- down_ready: bfloat16 [2048, 8192], P(None, 'tp')
All inputs are finite; a program needn't handle non-finite values.
Results may differ from a plain program's by a relative error of at most 0.0095.
Values may be sent and summed in bfloat16 or wider, within the bound.
A program may use at most 64 MiB of HBM per device.

v0:
```python
import jax
import jax.numpy as jnp
from jax import lax
from jax.sharding import Mesh
from jax.sharding import PartitionSpec as P

TP = ("tp_0", "tp_1")
FS_TP = ("fs", "tp_0", "tp_1")


def in_one_piece(arrays, axis, dim, along):
    both = jnp.concatenate(arrays, axis=along)
    whole, at, gathered = (lax.all_gather(both, axis, axis=dim, tiled=True), 0, [])
    for a in arrays:
        gathered.append(lax.slice_in_dim(whole, at, at + a.shape[along], axis=along))
        at += a.shape[along]
    return tuple(gathered)


def laid_out(parts, dim):
    dims = list(parts.shape[1:])
    dims[dim] *= parts.shape[0]
    return jnp.moveaxis(parts, 0, dim).reshape(dims)


def copy_for_each(array, axis):
    copies = jnp.broadcast_to(array, (lax.axis_size(axis), *array.shape))
    return lax.all_to_all(copies, axis, split_axis=0, concat_axis=0, tiled=True)


def collect(array, axis, dim):
    return laid_out(copy_for_each(array, axis), dim)


def own_block(parts, axes, sequence):
    inside = parts.shape[1:]
    parts = parts.reshape(*(lax.axis_size(a) for a in axes), *inside)
    parts = jnp.moveaxis(parts, sequence, range(len(axes))).reshape(-1, *inside)
    for k in sequence:
        parts = lax.psum_scatter(parts, axes[k], scatter_dimension=0, tiled=True)
    return parts[0]


def split_up(array, dim, length):
    dims = array.shape
    parts = array.reshape(*dims[:dim], length, dims[dim] // length, *dims[dim + 1 :])
    return jnp.moveaxis(parts, dim, 0)


def sum_by_axis(array, axes, sequence, dim):
    length = lax.axis_size(axes)
    return own_block(split_up(array, dim, length), axes, sequence)


def expand_rows(rows, gate_ready, up_ready):
    rows_wide = rows.astype(jnp.float32)
    row_scale = lax.rsqrt(jnp.mean(rows_wide * rows_wide, axis=1, keepdims=True) + 1e-06)
    gate_proj = row_scale * jnp.dot(rows, gate_ready, preferred_element_type=jnp.float32)
    up_proj = row_scale * jnp.dot(rows, up_ready, preferred_element_type=jnp.float32)
    return (jax.nn.silu(gate_proj) * up_proj).astype(jnp.bfloat16)


def body(tokens, norm_gain, gate_master, up_master, down_master):
    gate_local = (norm_gain[:, None] * gate_master).astype(jnp.bfloat16)
    up_local = (norm_gain[:, None] * up_master).astype(jnp.bfloat16)
    down_local = down_master.astype(jnp.bfloat16)
    gate_ready, up_ready = in_one_piece((gate_local, up_local), "fs", 0, 1)
    gathered = lax.all_gather(tokens, TP, axis=0, tiled=True)
    hidden = expand_rows(gathered, gate_ready, up_ready)
    down_ready = collect(down_local, "fs", 0)
    partial_value = lax.dot_general(
        hidden, down_ready, (((1,), (1,)), ((), ())), preferred_element_type=jnp.float32
    )
    summed = sum_by_axis(partial_value.astype(jnp.bfloat16), TP, (1, 0), 0).astype(jnp.float32)
    mixed = (tokens.astype(jnp.float32) + 0.5 * summed).astype(jnp.bfloat16)
    return (mixed, gate_ready, up_ready, down_ready)


def solution(mesh):
    split = Mesh(mesh.devices.reshape(mesh.shape["fs"], 16, 2), ("fs", "tp_0", "tp_1"))
    placed = (P(FS_TP, None), P("fs"), P("fs", TP), P("fs", TP), P("fs", TP))
    return jax.shard_map(
        body,
        mesh=split,
        in_specs=placed,
        out_specs=(P(FS_TP, None), P(None, TP), P(None, TP), P(None, TP)),
        check_vma=False,
    )
```

profile of v0, /device:TPU:6, one launch (start us, length us, event | category | flops | bytes accessed | tf_op | source)
XLA Modules:
  0.0 275.8 jit_solution(10192223352747149037)
XLA Ops:
  7.2 0.0 all-gather.5.cloned.1.call-start
  7.2 1.1 multiply_convert_fusion.1
  8.3 0.7 pad_maximum_fusion
  9.0 0.0 all-gather.5.cloned.1.call-update
  9.0 0.0 all-gather.3.cloned.1.call-start
  9.0 0.7 all-gather.3.cloned.1.call-update
  9.7 0.9 convert_element_type.33
  10.6 1.1 broadcast_in_dim.2
  11.7 9.3 %all-to-all-start = ((bf16[16,128,256]{2,1,0:T(8,128)(2,1)}), bf16[16,128,256]{2,1,0:T(8,128)(2,1)S(1)}, u32[]{:S(2)}, u32[]{:S(2)}) async-start(bf16[16,128,256]{2,1,0:T(8,128)(2,1)} %broadcast_in_dim.2), calls=%async_computation | async-start | bytes 2097152 | tf_op jit(solution)/shard_map/all_to_all | solution.py:28
  21.0 0.0 reduce-scatter.3.cloned.1.call-start
  21.0 54.8 %all-gather.5.cloned.1.call-done = bf16[2048,512]{1,0:T(8,128)(2,1)} async-done(((bf16[128,512]{1,0:T(8,128)(2,1)}), bf16[2048,512]{1,0:T(8,128)(2,1)}) %all-gather.5.cloned.1.call-update) | async-done | bytes 2097168 | tf_op jit(solution)/shard_map/all_gather | solution.py:13
  75.9 1.7 fusion.13
  77.6 73.6 %all-gather.3.cloned.1.call-done = bf16[1024,2048]{1,0:T(8,128)(2,1)} async-done(((bf16[32,2048]{1,0:T(8,128)(2,1)}), bf16[1024,2048]{1,0:T(8,128)(2,1)}) %all-gather.3.cloned.1.call-update) | async-done | bytes 4194320 | tf_op jit(solution)/shard_map/all_gather | solution.py:68
  151.2 3.2 %multiply_reduce_fusion = f32[1024]{0:T(1024)S(1)} fusion(bf16[1024,2048]{1,0:T(8,128)(2,1)} %all-gather.3.cloned.1.call-done), kind=kLoop, calls=%fused_computation | loop fusion | flops 6290432 | bytes 4198400 | tf_op jit(solution)/shard_map/reduce_sum | solution.py:57
  154.4 0.2 copy-done
  154.6 2.4 fusion.1
  157.0 7.0 %convolution_convert_fusion = bf16[1024,2048]{1,0:T(8,128)(2,1)} fusion(bf16[2048,256]{1,0:T(8,128)(2,1)S(1)} %bitcast.26, bf16[2048,256]{1,0:T(8,128)(2,1)S(1)} %get-tuple-element.14, bf16[1024,2048]{1,0:T(8,128)(2,1)} %all-gather.3.cloned.1.call-done, f32[1024,256]{0,1:T(8,128)} %fusion.1, f32[1024]{0:T(1024)S(1)} %add_rsqrt_fusion), kind=kOutput, calls=%fused_computation.1 | convolution fusion | flops 2151415808 | bytes 11538432 | tf_op jit(solution)/shard_map/dot_general | solution.py:71
  164.0 4.7 %copy.9 = bf16[2,16,32,2048]{3,2,1,0:T(8,128)(2,1)} copy(bf16[2,16,32,2048]{3,2,0,1:T(8,128)(2,1)} %bitcast.25) | data formatting | bytes 8388608 | tf_op jit(solution)/shard_map/transpose | solution.py:38
  168.8 0.0 reduce-scatter.3.cloned.1.call-update
  168.8 0.0 reduce-scatter.5.cloned.1.call-start
  168.9 19.5 %reduce-scatter.3.cloned.1.call-done = bf16[16,32,2048]{2,1,0:T(8,128)(2,1)} async-done(((bf16[32,32,2048]{2,1,0:T(8,128)(2,1)}), bf16[16,32,2048]{2,1,0:T(8,128)(2,1)}) %reduce-scatter.3.cloned.1.call-update) | async-done | bytes 2097168 | tf_op jit(solution)/shard_map/reduce_scatter | solution.py:40
  188.4 78.3 %reduce-scatter.5.cloned.1.call-done = bf16[1,32,2048]{2,1,0:T(8,128)(2,1)} async-done(((bf16[16,32,2048]{2,1,0:T(8,128)(2,1)}), bf16[1,32,2048]{2,1,0:T(8,128)(2,1)}) %reduce-scatter.5.cloned.1.call-update) | async-done | bytes 131088 | tf_op jit(solution)/shard_map/reduce_scatter | solution.py:40
  266.7 1.6 fusion.11
  268.3 1.0 copy.11
  (10 shorter events, 0.0 us)
Async XLA Ops:
  7.2 68.7 %all-gather.5.cloned.1.call-start = ((), (), s32[]{:S(2)}) async-start(), calls=%async_computation.4 | async-start | bytes 2228224 | tf_op jit(solution)/shard_map/all_gather | solution.py:13
  9.0 142.2 %all-gather.3.cloned.1.call-start = ((), (), s32[]{:S(2)}) async-start(), calls=%async_computation.3 | async-start | bytes 4325376 | tf_op jit(solution)/shard_map/all_gather | solution.py:68
  11.7 145.3 %all-to-all-start = ((bf16[16,128,256]{2,1,0:T(8,128)(2,1)}), bf16[16,128,256]{2,1,0:T(8,128)(2,1)S(1)}, u32[]{:S(2)}, u32[]{:S(2)}) async-start(bf16[16,128,256]{2,1,0:T(8,128)(2,1)} %broadcast_in_dim.2), calls=%async_computation | async-start | bytes 2097152 | tf_op jit(solution)/shard_map/all_to_all | solution.py:28
  21.0 167.4 %reduce-scatter.3.cloned.1.call-start = ((), (), s32[]{:S(2)}) async-start(), calls=%async_computation.5 | async-start | bytes 6291456 | tf_op jit(solution)/shard_map/reduce_scatter | solution.py:40
  77.6 79.4 %copy-start.1 = (bf16[2048,256]{1,0:T(8,128)(2,1)}, bf16[2048,256]{1,0:T(8,128)(2,1)S(1)}, u32[]{:S(2)}) copy-start(bf16[2048,256]{1,0:T(8,128)(2,1)S(1)} %get-tuple-element.13) | copy-start | bytes 3145732
  77.6 79.4 %copy-start.2 = (bf16[2048,256]{1,0:T(8,128)(2,1)}, bf16[2048,256]{1,0:T(8,128)(2,1)S(1)}, u32[]{:S(2)}) copy-start(bf16[2048,256]{1,0:T(8,128)(2,1)S(1)} %get-tuple-element.14) | copy-start | bytes 3145732
  151.2 3.4 %copy-start = (bf16[1024,2048]{1,0:T(8,128)(2,1)S(1)}, bf16[1024,2048]{1,0:T(8,128)(2,1)}, u32[]{:S(2)}) copy-start(bf16[1024,2048]{1,0:T(8,128)(2,1)} %all-gather.3.cloned.1.call-done) | copy-start | bytes 12582916
  168.8 97.9 %copy-start.3 = (bf16[32,2048]{1,0:T(8,128)(2,1)S(1)}, bf16[32,2048]{1,0:T(8,128)(2,1)}, u32[]{:S(2)}) copy-start(bf16[32,2048]{1,0:T(8,128)(2,1)} %param.5) | copy-start | bytes 393220
  168.8 97.9 %reduce-scatter.5.cloned.1.call-start = ((), (), s32[]{:S(2)}) async-start(), calls=%async_computation.6 | async-start | bytes 2228224 | tf_op jit(solution)/shard_map/reduce_scatter | solution.py:40
Sparse Core Ops, SparseCore 0:
  11.6 64.2 all-gather.4
  78.0 73.1 all-gather.2
  168.9 19.3 reduce-scatter.2
  191.0 75.5 reduce-scatter.4
where the time goes:
time: 276 us
  waiting for transfers between devices  227 us (82%)
  between operations  13.8 us (5%)
  starting transfers between devices  9.44 us (3%)
  matrix products  9.4 us (3%)
  local copies, waits for them, and re-layouts  8.68 us (3%)
  other arithmetic  7.48 us (3%)
    reduce_scatter x2, waiting for transfers between devices, own_block(): parts = lax.psum_scatter(parts, axes[k], scatter_dimension=0, tiled=True)  97.8 us
    all_gather x1, waiting for transfers between devices, body(): gathered = lax.all_gather(tokens, TP, axis=0, tiled=True)  73.6 us
    all_gather x1, waiting for transfers between devices, in_one_piece(): lax.all_gather(both, axis, axis=dim, tiled=True)  54.8 us
    all_to_all x1, starting transfers between devices, copy_for_each(): return lax.all_to_all(copies, axis, split_axis=0, concat_axis=0, tiled=True)  9.28 us
    dot_general x1, matrix products, body(): lax.dot_general(hidden, down_ready, (((1,), (1,)), ((), ())), preferred_e...  7.04 us
  transfers between devices with their start and end apart: 5, of which 4 were waited for; matrix products, arithmetic and copies ran while one was open for 3% of the time, Pallas kernels for 0%

commit v1 on v0

--- a/solution.py
+++ b/solution.py
@@ -65,7 +65,16 @@
     up_local = (norm_gain[:, None] * up_master).astype(jnp.bfloat16)
     down_local = down_master.astype(jnp.bfloat16)
     gate_ready, up_ready = in_one_piece((gate_local, up_local), "fs", 0, 1)
-    gathered = lax.all_gather(tokens, TP, axis=0, tiled=True)
+    screen_return_all = lambda mat, peer_axis, array_axis: jnp.concatenate(
+        lax.all_to_all(
+            jnp.stack(lax.axis_size(peer_axis) * [mat], axis=0),
+            split_axis=0,
+            axis_name=peer_axis,
+            concat_axis=0,
+        ),
+        axis=array_axis,
+    )
+    gathered = screen_return_all(tokens, TP, 0)
     hidden = expand_rows(gathered, gate_ready, up_ready)
     down_ready = collect(down_local, "fs", 0)
     partial_value = lax.dot_general(

time: 276 us -> 353 us (1.28)
  waiting for transfers between devices: 227 us -> 286 us
  starting transfers between devices: 9.44 us -> 23.3 us
    all_to_all x0 -> x1, waiting for transfers between devices: none -> 116 us  [body(): lax.all_to_all(jnp.stack(lax.axis_size(peer_axis) * [mat], axis=0), split...]
    all_gather x1 -> x0, waiting for transfers between devices: 73.6 us -> none  [body(): gathered = lax.all_gather(tokens, TP, axis=0, tiled=True)]
    all_to_all x0 -> x1, starting transfers between devices: none -> 15.8 us  [body(): lax.all_to_all(jnp.stack(lax.axis_size(peer_axis) * [mat], axis=0), split...]
    all_gather x1, waiting for transfers between devices: 54.8 us -> 64.5 us  [in_one_piece(): lax.all_gather(both, axis, axis=dim, tiled=True)]
    all_to_all x1, waiting for transfers between devices: 0.01 us -> 6.99 us  [copy_for_each(): return lax.all_to_all(copies, axis, split_axis=0, concat_axis=0, tiled=True)]
  transfers between devices with their start and end apart: 5 -> 5, of which waited for: 4 -> 5; matrix products, arithmetic and copies ran while one was open for 3% -> 3% of each run, Pallas kernels for 0% -> 0%
where the time goes in v1:
time: 353 us
  waiting for transfers between devices  286 us (81%)
  starting transfers between devices  23.3 us (7%)
  between operations  13.8 us (4%)
  local copies, waits for them, and re-layouts  11.9 us (3%)
  matrix products  11.6 us (3%)
  other arithmetic  5.44 us (2%)
    all_to_all x1, waiting for transfers between devices, body(): lax.all_to_all(jnp.stack(lax.axis_size(peer_axis) * [mat], axis=0), split...  116 us
    reduce_scatter x2, waiting for transfers between devices, own_block(): parts = lax.psum_scatter(parts, axes[k], scatter_dimension=0, tiled=True)  98.5 us
    all_gather x1, waiting for transfers between devices, in_one_piece(): lax.all_gather(both, axis, axis=dim, tiled=True)  64.5 us
    all_to_all x1, starting transfers between devices, body(): lax.all_to_all(jnp.stack(lax.axis_size(peer_axis) * [mat], axis=0), split...  15.8 us
    all_to_all x1, starting transfers between devices, copy_for_each(): return lax.all_to_all(copies, axis, split_axis=0, concat_axis=0, tiled=True)  7.42 us
  transfers between devices with their start and end apart: 5, of which 5 were waited for; matrix products, arithmetic and copies ran while one was open for 3% of the time, Pallas kernels for 0%

profile of v1, /device:TPU:6, one launch (start us, length us, event | category | flops | bytes accessed | tf_op | source)
XLA Modules:
  0.0 352.6 jit_solution(9775286297000736503)
XLA Ops:
  7.2 3.4 stack.2
  10.6 15.8 %all-to-all-start = ((bf16[32,32,2048]{2,1,0:T(8,128)(2,1)}), bf16[32,32,2048]{2,1,0:T(8,128)(2,1)}, u32[]{:S(2)}, u32[]{:S(2)}) async-start(bf16[32,32,2048]{2,1,0:T(8,128)(2,1)} %stack.2), calls=%async_computation | async-start | bytes 8388608 | tf_op jit(solution)/shard_map/all_to_all | solution.py:69
  26.3 0.0 all-gather.2.cloned.1.call-start
  26.4 0.1 multiply_convert_fusion.1
  26.5 0.7 pad_maximum_fusion
  27.2 0.0 all-gather.2.cloned.1.call-update
  27.2 64.5 %all-gather.2.cloned.1.call-done = bf16[2048,512]{1,0:T(8,128)(2,1)} async-done(((bf16[128,512]{1,0:T(8,128)(2,1)}), bf16[2048,512]{1,0:T(8,128)(2,1)}) %all-gather.2.cloned.1.call-update) | async-done | bytes 2097168 | tf_op jit(solution)/shard_map/all_gather | solution.py:13
  91.7 1.7 fusion.13
  93.4 116.4 %all-to-all-done = bf16[32,32,2048]{2,1,0:T(8,128)(2,1)} async-done(((bf16[32,32,2048]{2,1,0:T(8,128)(2,1)}), bf16[32,32,2048]{2,1,0:T(8,128)(2,1)}, u32[]{:S(2)}, u32[]{:S(2)}) %all-to-all-start) | async-done | bytes 4194336 | tf_op jit(solution)/shard_map/all_to_all | solution.py:69
  209.8 1.1 broadcast_in_dim.2
  210.9 7.4 %all-to-all-start.1 = ((bf16[16,128,256]{2,1,0:T(8,128)(2,1)}), bf16[16,128,256]{2,1,0:T(8,128)(2,1)S(1)}, u32[]{:S(2)}, u32[]{:S(2)}) async-start(bf16[16,128,256]{2,1,0:T(8,128)(2,1)} %broadcast_in_dim.2), calls=%async_computation.1 | async-start | bytes 2097152 | tf_op jit(solution)/shard_map/all_to_all | solution.py:28
  218.3 0.0 reduce-scatter.3.cloned.1.call-start
  218.4 3.1 multiply_reduce_fusion
  221.5 0.1 rsqrt.12
  221.5 4.6 %fusion.1 = f32[1024,256]{0,1:T(8,128)} fusion(bf16[2048,256]{1,0:T(8,128)(2,1)S(1)} %get-tuple-element.13, bf16[1024,2048]{1,0:T(8,128)(2,1)} %bitcast, f32[1024]{0:T(1024)S(1)} %rsqrt.12), kind=kOutput, calls=%fused_computation.5 | convolution fusion | flops 1074003968 | bytes 6295552 | tf_op jit(solution)/shard_map/dot_general | solution.py:58
  226.1 7.0 %all-to-all-done.1 = bf16[16,128,256]{2,1,0:T(8,128)(2,1)S(1)} async-done(((bf16[16,128,256]{2,1,0:T(8,128)(2,1)}), bf16[16,128,256]{2,1,0:T(8,128)(2,1)S(1)}, u32[]{:S(2)}, u32[]{:S(2)}) %all-to-all-start.1) | async-done | bytes 1048608 | tf_op jit(solution)/shard_map/all_to_all | solution.py:28
  233.1 7.0 %convolution_convert_fusion = bf16[1024,2048]{1,0:T(8,128)(2,1)} fusion(bf16[2048,256]{1,0:T(8,128)(2,1)S(1)} %bitcast.27, bf16[2048,256]{1,0:T(8,128)(2,1)S(1)} %get-tuple-element.14, bf16[1024,2048]{1,0:T(8,128)(2,1)} %bitcast, f32[1024,256]{0,1:T(8,128)} %fusion.1, f32[1024]{0:T(1024)S(1)} %rsqrt.12), kind=kOutput, calls=%fused_computation.1 | convolution fusion | flops 2151415808 | bytes 11538432 | tf_op jit(solution)/shard_map/dot_general | solution.py:80
  240.1 4.7 %copy.10 = bf16[2,16,32,2048]{3,2,1,0:T(8,128)(2,1)} copy(bf16[2,16,32,2048]{3,2,0,1:T(8,128)(2,1)} %bitcast.26) | data formatting | bytes 8388608 | tf_op jit(solution)/shard_map/transpose | solution.py:38
  244.9 0.0 reduce-scatter.5.cloned.1.call-start
  244.9 20.0 %reduce-scatter.3.cloned.1.call-done = bf16[16,32,2048]{2,1,0:T(8,128)(2,1)} async-done(((bf16[32,32,2048]{2,1,0:T(8,128)(2,1)}), bf16[16,32,2048]{2,1,0:T(8,128)(2,1)}) %reduce-scatter.3.cloned.1.call-update) | async-done | bytes 2097168 | tf_op jit(solution)/shard_map/reduce_scatter | solution.py:40
  265.0 0.0 reduce-scatter.5.cloned.1.call-update
  265.0 78.5 %reduce-scatter.5.cloned.1.call-done = bf16[1,32,2048]{2,1,0:T(8,128)(2,1)} async-done(((bf16[16,32,2048]{2,1,0:T(8,128)(2,1)}), bf16[1,32,2048]{2,1,0:T(8,128)(2,1)}) %reduce-scatter.5.cloned.1.call-update) | async-done | bytes 131088 | tf_op jit(solution)/shard_map/reduce_scatter | solution.py:40
  343.5 1.6 fusion.11
  345.1 1.0 copy.12
  (17 shorter events, 0.1 us)
Async XLA Ops:
  10.6 15.8 %copy-start.4 = (f32[128,256]{1,0:T(8,128)S(1)}, f32[128,256]{1,0:T(8,128)}, u32[]{:S(2)}) copy-start(f32[128,256]{1,0:T(8,128)} %param.7) | copy-start | bytes 393220
  10.6 15.8 %copy-start.5 = (f32[128,256]{1,0:T(8,128)S(1)}, f32[128,256]{1,0:T(8,128)}, u32[]{:S(2)}) copy-start(f32[128,256]{1,0:T(8,128)} %param.8) | copy-start | bytes 393220
  10.6 15.8 %copy-start.6 = (f32[128]{0:T(128)S(1)}, f32[128]{0:T(128)}, u32[]{:S(2)}) copy-start(f32[128]{0:T(128)} %param.6) | copy-start | bytes 1540
  10.6 16.6 %copy-start.3 = (f32[128,256]{1,0:T(8,128)S(1)}, f32[128,256]{1,0:T(8,128)}, u32[]{:S(2)}) copy-start(f32[128,256]{1,0:T(8,128)} %param.9) | copy-start | bytes 393220
  10.6 199.3 %all-to-all-start = ((bf16[32,32,2048]{2,1,0:T(8,128)(2,1)}), bf16[32,32,2048]{2,1,0:T(8,128)(2,1)}, u32[]{:S(2)}, u32[]{:S(2)}) async-start(bf16[32,32,2048]{2,1,0:T(8,128)(2,1)} %stack.2), calls=%async_computation | async-start | bytes 8388608 | tf_op jit(solution)/shard_map/all_to_all | solution.py:69
  26.3 65.3 %all-gather.2.cloned.1.call-start = ((), (), s32[]{:S(2)}) async-start(), calls=%async_computation.4 | async-start | bytes 2228224 | tf_op jit(solution)/shard_map/all_gather | solution.py:13
  93.4 132.7 %copy-start = (bf16[2048,256]{1,0:T(8,128)(2,1)}, bf16[2048,256]{1,0:T(8,128)(2,1)S(1)}, u32[]{:S(2)}) copy-start(bf16[2048,256]{1,0:T(8,128)(2,1)S(1)} %get-tuple-element.13) | copy-start | bytes 3145732
  93.4 139.7 %copy-start.1 = (bf16[2048,256]{1,0:T(8,128)(2,1)}, bf16[2048,256]{1,0:T(8,128)(2,1)S(1)}, u32[]{:S(2)}) copy-start(bf16[2048,256]{1,0:T(8,128)(2,1)S(1)} %get-tuple-element.14) | copy-start | bytes 3145732
  210.9 22.2 %all-to-all-start.1 = ((bf16[16,128,256]{2,1,0:T(8,128)(2,1)}), bf16[16,128,256]{2,1,0:T(8,128)(2,1)S(1)}, u32[]{:S(2)}, u32[]{:S(2)}) async-start(bf16[16,128,256]{2,1,0:T(8,128)(2,1)} %broadcast_in_dim.2), calls=%async_computation.1 | async-start | bytes 2097152 | tf_op jit(solution)/shard_map/all_to_all | solution.py:28
  218.3 46.6 %reduce-scatter.3.cloned.1.call-start = ((), (), s32[]{:S(2)}) async-start(), calls=%async_computation.5 | async-start | bytes 6291456 | tf_op jit(solution)/shard_map/reduce_scatter | solution.py:40
  244.9 98.6 %copy-start.2 = (bf16[32,2048]{1,0:T(8,128)(2,1)S(1)}, bf16[32,2048]{1,0:T(8,128)(2,1)}, u32[]{:S(2)}) copy-start(bf16[32,2048]{1,0:T(8,128)(2,1)} %param.5) | copy-start | bytes 393220
  244.9 98.6 %reduce-scatter.5.cloned.1.call-start = ((), (), s32[]{:S(2)}) async-start(), calls=%async_computation.6 | async-start | bytes 2228224 | tf_op jit(solution)/shard_map/reduce_scatter | solution.py:40
Sparse Core Ops, SparseCore 0:
  30.7 60.9 all-gather.1
  245.0 19.9 reduce-scatter.2
  267.8 75.6 reduce-scatter.4
